TPU v7x, 512 devices: a whole 4x8x8 slice. The times are simulated.
512 devices in a mesh: ep: 128 (over z, y, core), tp: 4 (over x).
Axes of the slice: x: 4, y: 8, z: 8, core: 2. Of those that a mesh axis runs over, the one named last changes fastest.
Arguments:
- tokens: bfloat16 [2048, 1024], P(('ep', 'tp')), may hold values from -6 to 6
- lengths: int32 [2048], P('ep'), may hold values from 256 to 1024
- key_cache: bfloat16 [2048, 1024, 128], P(('ep', 'tp')), may hold values from -1500 to 1500
- value_cache: bfloat16 [2048, 1024, 128], P(('ep', 'tp')), may hold values from -6 to 6
- query_weight: bfloat16 [1024, 512], P(None, 'tp'), may hold values from -0.1875 to 0.1875
- key_weight: bfloat16 [1024, 128], replicated, may hold values from -0.1875 to 0.1875
- value_weight: bfloat16 [1024, 128], replicated, may hold values from -0.1875 to 0.1875
- lambdas: float32 [4], replicated, may hold values from 0.3 to 0.8
- head_gain: float32 [128], replicated, may hold values from 0.1 to 1.9
- output_weight: bfloat16 [512, 1024], P(None, 'tp'), may hold values from -0.25 to 0.25
- norm1_gain: float32 [1024], replicated, may hold values from 0.1 to 1.9
- routes: int32 [2048, 6], P('ep'), may hold values from 0 to 127, all different within a row; in each aligned block of 16 rows (0 to 15, 16 to 31, ...) at most 2 rows name the same one
- route_logits: float32 [2048, 6], P('ep'), may hold values from -9 to 410
- gate_weight: bfloat16 [128, 1024, 1024], P('ep', None, 'tp'), may hold values from -0.5 to 0.5
- up_weight: bfloat16 [128, 1024, 1024], P('ep', None, 'tp'), may hold values from -0.5 to 0.5
- down_weight: bfloat16 [128, 1024, 1024], P('ep', 'tp'), may hold values from -0.09375 to 0.09375
- norm2_gain: float32 [1024], replicated, may hold values from 0.1 to 1.9
Outputs:
- mixed: bfloat16 [2048, 1024], P('ep', 'tp')
Inputs may be any that keep to these rules, and one draw needn't show every extreme that they name: `routes`: in the 16 rows of each aligned block (the rows held by one index of ep) no expert is named by more than 2 rows, a bound that some block reaches; the experts of a row differ.
All inputs are finite; a program needn't handle non-finite values.
Results may differ from a plain program's by a relative error of at most 0.014.
Values may be sent and summed in bfloat16 or wider, within the bound.
A program may use at most 64 MiB of HBM per device.

v0:
```python
import jax
import jax.numpy as jnp
from jax import lax
from jax.sharding import PartitionSpec as P

ALPHA = 1.4142135623730951
EPS = 1e-05
THETA = 500000.0
LIMIT = 7.0
SLOPE = 1.702


def copy_for_each(x, axis):
    count = lax.axis_size(axis)
    return lax.all_to_all(jnp.broadcast_to(x[None], (count, *x.shape)), axis, 0, 0, tiled=True)


def in_order(pieces, dim):
    lengths = list(pieces.shape[1:])
    lengths[dim] *= pieces.shape[0]
    return jnp.moveaxis(pieces, 0, dim).reshape(lengths)


def gathered_copies(x, axis, dim):
    pieces = copy_for_each(x, axis)
    return in_order(pieces, dim)


def split_up(x, dim, count):
    lengths = x.shape
    pieces = x.reshape(*lengths[:dim], count, lengths[dim] // count, *lengths[dim + 1 :])
    return jnp.moveaxis(pieces, dim, 0)


def sum_at_owner(x, axis, dim):
    pieces = split_up(x, dim, lax.axis_size(axis))
    arrived = lax.all_to_all(pieces, axis, split_axis=0, concat_axis=0, tiled=True)
    return arrived.astype(jnp.float32).sum(axis=0)


def over_copies(x, axis):
    everything = copy_for_each(x, axis)
    return jnp.sum(everything, axis=0)


def packed_total(arrays, axis):
    ends = [0]
    for a in arrays:
        ends.append(ends[-1] + a.size)
    subtotal = over_copies(jnp.concatenate([a.ravel() for a in arrays]), axis)
    return tuple((subtotal[b:e].reshape(a.shape) for a, b, e in zip(arrays, ends, ends[1:])))


def rotate(values, positions):
    half = values.shape[-1] // 2
    freqs = THETA ** (-jnp.arange(half, dtype=jnp.float32) / half)
    angles = positions.astype(jnp.float32)[:, None] * freqs[None, :]
    shape = (angles.shape[0],) + (1,) * (values.ndim - 2) + (half,)
    cosine = jnp.cos(angles).reshape(shape)
    sine = jnp.sin(angles).reshape(shape)
    first = values[..., :half]
    second = values[..., half:]
    return jnp.concatenate(
        [first * cosine - second * sine, second * cosine + first * sine], axis=-1
    )


def norm_rows(summed, gain):
    mean = jnp.mean(summed, axis=-1, keepdims=True)
    center = summed - mean
    spread = jnp.mean(center * center, axis=-1, keepdims=True)
    return center * lax.rsqrt(spread + EPS) * gain


def scaled_part(summed, sums, squares, width, gain):
    mean = sums / width
    spread = squares / width - mean * mean
    return (summed - mean[:, None]) * lax.rsqrt(spread + EPS)[:, None] * gain


def choose_slots(routes_block, experts, capacity):
    flat = routes_block.reshape(-1)
    onehot = (flat[:, None] == jnp.arange(experts, dtype=jnp.int32)[None, :]).astype(jnp.int32)
    before = jnp.cumsum(onehot, axis=0) - onehot
    slot = jnp.sum(before * onehot, axis=1)
    target = flat * capacity + slot
    return target[:, None] == jnp.arange(experts * capacity, dtype=jnp.int32)[None, :]


def body(
    tokens,
    lengths,
    key_cache,
    value_cache,
    query_weight,
    key_weight,
    value_weight,
    lambdas,
    head_gain,
    output_weight,
    norm1_gain,
    routes,
    route_logits,
    gate_weight,
    up_weight,
    down_weight,
    norm2_gain,
):
    bf16 = jnp.bfloat16
    f32 = jnp.float32
    tp_count = lax.axis_size("tp")
    tp_rank = lax.axis_index("tp")
    own, width = tokens.shape
    group = own * tp_count
    part = width // tp_count
    heads = lambdas.shape[0]
    head_dim = key_weight.shape[1] // 2
    length = key_cache.shape[1]
    group_rows = gathered_copies(tokens, "tp", 0)
    query = jnp.dot(group_rows, query_weight, preferred_element_type=f32).reshape(
        group, -1, 2, head_dim
    )
    query = rotate(query, lengths).astype(bf16).reshape(group, -1)
    query = lax.all_to_all(query, "tp", split_axis=0, concat_axis=1, tiled=True).reshape(
        own, heads, 2, head_dim
    )
    own_lengths = lax.dynamic_slice_in_dim(lengths, tp_rank * own, own)
    new_key = jnp.dot(tokens, key_weight, preferred_element_type=f32).reshape(own, 2, head_dim)
    new_key = rotate(new_key, own_lengths).astype(bf16)
    new_value = jnp.dot(tokens, value_weight, preferred_element_type=f32).astype(bf16)
    keys = key_cache.reshape(own, length, 2, head_dim)
    scale = head_dim ** (-0.5)
    past = jnp.einsum("bhmd,bjmd->bhmj", query, keys, preferred_element_type=f32) * scale
    live = jnp.arange(length, dtype=jnp.int32)[None, :] < own_lengths[:, None]
    past = jnp.where(live[:, None, None, :], past, -jnp.inf)
    selfs = jnp.einsum("bhmd,bmd->bhm", query, new_key, preferred_element_type=f32) * scale
    top = jnp.maximum(jnp.max(past, axis=-1), selfs)
    past_exp = jnp.exp(past - top[..., None])
    self_exp = jnp.exp(selfs - top)
    total = jnp.sum(past_exp, axis=-1) + self_exp
    past_prob = past_exp / total[..., None]
    self_prob = self_exp / total
    mixing = lambdas[None, :]
    past_weight = (past_prob[:, :, 0] - mixing[..., None] * past_prob[:, :, 1]).astype(bf16)
    self_weight = (self_prob[:, :, 0] - mixing * self_prob[:, :, 1]).astype(bf16)
    head_out = jnp.einsum("bhj,bje->bhe", past_weight, value_cache, preferred_element_type=f32)
    head_out = head_out + self_weight.astype(f32)[..., None] * new_value.astype(f32)[:, None, :]
    normed = (
        head_out
        * lax.rsqrt(jnp.mean(head_out * head_out, axis=-1, keepdims=True) + EPS)
        * head_gain
    )
    attended = normed.astype(bf16).reshape(own, -1)
    mix = jnp.dot(gathered_copies(attended, "tp", 0), output_weight, preferred_element_type=f32)
    column_start = tp_rank * part
    own_columns = lax.dynamic_slice_in_dim(group_rows, column_start, part, 1).astype(f32)
    summed = ALPHA * own_columns + mix
    whole = gathered_copies(summed, "tp", 1)
    settled = norm_rows(whole, norm1_gain).astype(bf16)
    settled_part = lax.dynamic_slice_in_dim(settled, column_start, part, 1)
    experts = lax.axis_size("ep")
    topk = routes.shape[1]
    capacity = min(group, max(2, 2 * group * topk // experts))
    chosen = choose_slots(routes, experts, capacity)
    placing = jnp.sum(chosen.reshape(group, topk, -1).astype(f32), axis=1).astype(bf16)
    route_weight = jax.nn.softmax(route_logits, axis=-1)
    gate_local = gate_weight[0]
    up_local = up_weight[0]
    down_local = down_weight[0]
    outgoing = lax.dot_general(
        placing, settled, (((0,), (0,)), ((), ())), preferred_element_type=f32
    )
    outgoing = outgoing.astype(bf16).reshape(experts, capacity, width)
    rows = lax.all_to_all(outgoing, "ep", split_axis=0, concat_axis=0, tiled=True)
    gate_h = jnp.einsum("scd,df->scf", rows, gate_local, preferred_element_type=f32)
    up_h = jnp.einsum("scd,df->scf", rows, up_local, preferred_element_type=f32)
    clipped = jnp.minimum(gate_h, LIMIT)
    linear = jnp.clip(up_h, -LIMIT, LIMIT)
    act = (clipped * jax.nn.sigmoid(SLOPE * clipped) * (linear + 1.0)).astype(bf16)
    terms = jnp.einsum("scf,fd->scd", act, down_local, preferred_element_type=f32)
    answers = sum_at_owner(terms.astype(jnp.bfloat16), "tp", 2).astype(bf16)
    selector = chosen.astype(bf16)
    back = lax.all_to_all(answers, "ep", split_axis=0, concat_axis=0, tiled=True)
    picked = jnp.dot(selector, back.reshape(experts * capacity, -1), preferred_element_type=f32)
    routed = jnp.sum(picked.reshape(group, topk, -1) * route_weight[:, :, None], axis=1)
    final = ALPHA * settled_part.astype(f32) + routed
    sums, squares = packed_total((jnp.sum(final, axis=1), jnp.sum(final * final, axis=1)), "tp")
    gain_part = lax.dynamic_slice_in_dim(norm2_gain, column_start, part)
    result = scaled_part(final, sums, squares, width, gain_part).astype(bf16)
    return result


def solution(mesh):
    in_specs = (
        P(("ep", "tp"), None),
        P("ep"),
        P(("ep", "tp"), None, None),
        P(("ep", "tp"), None, None),
        P(None, "tp"),
        P(),
        P(),
        P(),
        P(),
        P(None, "tp"),
        P(),
        P("ep", None),
        P("ep", None),
        P("ep", None, "tp"),
        P("ep", None, "tp"),
        P("ep", "tp", None),
        P(),
    )
    out_specs = P("ep", "tp")
    return jax.shard_map(body, mesh=mesh, in_specs=in_specs, out_specs=out_specs, check_vma=False)
```

profile of v0, /device:TPU:1, one launch (start us, length us, event | category | flops | bytes accessed | tf_op | source)
XLA Modules:
  0.0 130.2 jit_solution(14348994020305583358)
XLA Ops:
  0.0 1.5 %broadcast_in_dim.22 = bf16[4,4,1024]{2,1,0:T(4,128)(2,1)} broadcast(bf16[4,1024]{1,0:T(4,128)(2,1)} %param.17), dimensions={1,2} | broadcast | bytes 40960 | tf_op jit(solution)/shard_map/broadcast_in_dim | solution.py:15
  1.5 4.8 %all-to-all-start = ((bf16[4,4,1024]{2,1,0:T(4,128)(2,1)}), bf16[4,4,1024]{2,1,0:T(4,128)(2,1)S(1)}, u32[]{:S(2)}, u32[]{:S(2)}) async-start(bf16[4,4,1024]{2,1,0:T(4,128)(2,1)} %broadcast_in_dim.22), calls=%async_computation | async-start | bytes 65536 | tf_op jit(solution)/shard_map/all_to_all | solution.py:15
  6.3 0.7 convert_element_type.67
  7.0 0.7 fusion.54
  7.7 1.1 fusion.56
  8.8 0.1 reshape.269
  8.9 0.1 multiply_cosine_fusion.1
  9.0 0.1 multiply_cosine_fusion
  9.2 0.8 fusion.6
  10.1 0.8 copy.109
  10.8 0.1 eq.51
  10.9 0.1 fusion.34
  11.0 0.1 reduce_window_sum.11
  11.2 0.2 select_reduce_fusion
  11.4 1.1 copy.102
  12.5 0.2 convolution_bitcast_fusion
  12.7 0.1 subtract_convert_fusion
  12.8 0.1 pad_maximum_fusion
  12.9 0.7 convert_element_type.68
  13.6 4.2 %all-to-all-start.1 = ((bf16[4,4,128]{2,1,0:T(4,128)(2,1)}), bf16[4,4,128]{2,1,0:T(4,128)(2,1)S(1)}, u32[]{:S(2)}, u32[]{:S(2)}) async-start(bf16[4,4,128]{2,1,0:T(4,128)(2,1)} %convert_element_type.68), calls=%async_computation.1 | async-start | bytes 8192 | tf_op jit(solution)/shard_map/all_to_all | solution.py:124
  17.9 0.5 copy.105
  18.5 0.1 reduce_sum.118
  18.5 0.1 copy.110
  18.6 3.4 %all-to-all-done.1 = bf16[4,4,128]{2,1,0:T(4,128)(2,1)S(1)} async-done(((bf16[4,4,128]{2,1,0:T(4,128)(2,1)}), bf16[4,4,128]{2,1,0:T(4,128)(2,1)S(1)}, u32[]{:S(2)}, u32[]{:S(2)}) %all-to-all-start.1) | async-done | bytes 4128 | tf_op jit(solution)/shard_map/all_to_all | solution.py:124
  22.0 0.1 reshape.284
  22.1 0.1 fusion.38
  22.2 0.3 fusion.55
  22.5 0.2 fusion.25
  22.8 0.1 fusion.24
  22.9 0.6 copy-done.7
  23.6 0.4 multiply_reduce_fusion.1
  24.0 0.7 copy-done.8
  24.7 0.6 broadcast_in_dim.26
  25.4 3.4 %all-to-all-start.2 = ((bf16[4,4,512]{2,1,0:T(4,128)(2,1)}), bf16[4,4,512]{2,1,0:T(4,128)(2,1)S(1)}, u32[]{:S(2)}, u32[]{:S(2)}) async-start(bf16[4,4,512]{2,1,0:T(4,128)(2,1)} %broadcast_in_dim.26), calls=%async_computation.2 | async-start | bytes 32768 | tf_op jit(solution)/shard_map/all_to_all | solution.py:15
  28.8 4.1 %all-to-all-done.2 = bf16[4,4,512]{2,1,0:T(4,128)(2,1)S(1)} async-done(((bf16[4,4,512]{2,1,0:T(4,128)(2,1)}), bf16[4,4,512]{2,1,0:T(4,128)(2,1)S(1)}, u32[]{:S(2)}, u32[]{:S(2)}) %all-to-all-start.2) | async-done | bytes 16416 | tf_op jit(solution)/shard_map/all_to_all | solution.py:15
  32.9 0.1 convolution_add_fusion
  33.1 0.6 broadcast_in_dim.27
  33.7 3.3 %all-to-all-start.3 = ((f32[4,16,256]{2,1,0:T(8,128)}), f32[4,16,256]{2,1,0:T(8,128)S(1)}, u32[]{:S(2)}, u32[]{:S(2)}) async-start(f32[4,16,256]{2,1,0:T(8,128)} %broadcast_in_dim.27), calls=%async_computation.3 | async-start | bytes 131072 | tf_op jit(solution)/shard_map/all_to_all | solution.py:15
  37.0 0.1 convert_reduce_fusion
  37.1 4.4 %all-to-all-done.3 = f32[4,16,256]{2,1,0:T(8,128)S(1)} async-done(((f32[4,16,256]{2,1,0:T(8,128)}), f32[4,16,256]{2,1,0:T(8,128)S(1)}, u32[]{:S(2)}, u32[]{:S(2)}) %all-to-all-start.3) | async-done | bytes 65568 | tf_op jit(solution)/shard_map/all_to_all | solution.py:15
  41.4 0.1 reduce_sum.115
  41.6 0.2 fusion.32
  41.8 0.7 copy-done.6
  42.6 0.3 convolution_convert_fusion.1
  42.9 0.2 reshape.272
  43.1 42.4 %all_to_all.49 = bf16[128,2,1024]{2,1,0:T(2,128)(2,1)S(1)} all-to-all(bf16[128,2,1024]{2,1,0:T(2,128)(2,1)S(1)} %reshape.272), channel_id=1, replica_groups=mesh['ep'=128,'tp'=4] {'ep'}, dimensions={0} | all-to-all | bytes 1048576 | tf_op jit(solution)/shard_map/all_to_all | solution.py:174
  85.5 0.3 convolution_minimum_fusion
  85.8 0.7 copy-done.10
  86.5 0.2 copy-done.11
  86.7 0.7 convolution_convert_fusion
  87.4 0.8 copy.141
  88.2 3.6 %all-to-all-start.5 = ((bf16[4,128,2,256]{3,1,2,0:T(8,128)(2,1)}), bf16[4,128,2,256]{3,1,2,0:T(8,128)(2,1)S(1)}, u32[]{:S(2)}, u32[]{:S(2)}) async-start(bf16[4,128,2,256]{3,1,2,0:T(8,128)(2,1)} %bitcast.101), calls=%async_computation.5 | async-start | bytes 1048576 | tf_op jit(solution)/shard_map/all_to_all | solution.py:37
  91.9 9.8 %all-to-all-done.5 = bf16[4,128,2,256]{3,1,2,0:T(8,128)(2,1)S(1)} async-done(((bf16[4,128,2,256]{3,1,2,0:T(8,128)(2,1)}), bf16[4,128,2,256]{3,1,2,0:T(8,128)(2,1)S(1)}, u32[]{:S(2)}, u32[]{:S(2)}) %all-to-all-start.5) | async-done | bytes 524320 | tf_op jit(solution)/shard_map/all_to_all | solution.py:37
  101.6 0.1 reduce_sum.120
  101.7 0.8 copy.115
  102.5 5.8 %all-to-all-start.6 = ((bf16[128,2,256]{2,1,0:T(2,128)(2,1)}), bf16[128,2,256]{2,1,0:T(2,128)(2,1)S(1)}, u32[]{:S(2)}, u32[]{:S(2)}) async-start(bf16[128,2,256]{2,1,0:T(2,128)(2,1)} %copy.115), calls=%async_computation.6 | async-start | bytes 262144 | tf_op jit(solution)/shard_map/all_to_all | solution.py:183
  108.3 12.8 %all-to-all-done.6 = bf16[128,2,256]{2,1,0:T(2,128)(2,1)S(1)} async-done(((bf16[128,2,256]{2,1,0:T(2,128)(2,1)}), bf16[128,2,256]{2,1,0:T(2,128)(2,1)S(1)}, u32[]{:S(2)}, u32[]{:S(2)}) %all-to-all-start.6) | async-done | bytes 131104 | tf_op jit(solution)/shard_map/all_to_all | solution.py:183
  121.2 0.2 fusion.5
  121.4 0.1 fusion.47
  121.6 0.6 broadcast_in_dim.28
  122.2 3.2 %all-to-all-start.7 = ((f32[4,1,32]{2,1,0:T(1,128)}), f32[4,1,32]{2,1,0:T(1,128)S(1)}, u32[]{:S(2)}, u32[]{:S(2)}) async-start(f32[4,1,32]{2,1,0:T(1,128)} %broadcast_in_dim.28), calls=%async_computation.7 | async-start | bytes 4096 | tf_op jit(solution)/shard_map/all_to_all | solution.py:15
  125.4 0.8 dynamic_slice.15
  126.2 3.3 %all-to-all-done.7 = f32[4,1,32]{2,1,0:T(1,128)S(1)} async-done(((f32[4,1,32]{2,1,0:T(1,128)}), f32[4,1,32]{2,1,0:T(1,128)S(1)}, u32[]{:S(2)}, u32[]{:S(2)}) %all-to-all-start.7) | async-done | bytes 544 | tf_op jit(solution)/shard_map/all_to_all | solution.py:15
  129.5 0.7 multiply_convert_fusion.1
  (46 shorter events, 0.8 us)
Async XLA Ops:
  0.0 23.6 %copy-start = (bf16[4,1024,128]{2,1,0:T(8,128)(2,1)S(1)}, bf16[4,1024,128]{2,1,0:T(8,128)(2,1)}, u32[]{:S(2)}) copy-start(bf16[4,1024,128]{2,1,0:T(8,128)(2,1)} %param.20) | copy-start | bytes 3145732
  0.0 9.2 %copy-start.3 = (bf16[1024,128]{1,0:T(8,128)(2,1)S(1)}, bf16[1024,128]{1,0:T(8,128)(2,1)}, u32[]{:S(2)}) copy-start(bf16[1024,128]{1,0:T(8,128)(2,1)} %param.23) | copy-start | bytes 786436
  0.0 17.9 %copy-start.1 = (bf16[4,1024,128]{2,1,0:T(8,128)(2,1)S(1)}, bf16[4,1024,128]{2,1,0:T(8,128)(2,1)}, u32[]{:S(2)}) copy-start(bf16[4,1024,128]{2,1,0:T(8,128)(2,1)} %param.19) | copy-start | bytes 3145732
  1.5 11.0 %all-to-all-start = ((bf16[4,4,1024]{2,1,0:T(4,128)(2,1)}), bf16[4,4,1024]{2,1,0:T(4,128)(2,1)S(1)}, u32[]{:S(2)}, u32[]{:S(2)}) async-start(bf16[4,4,1024]{2,1,0:T(4,128)(2,1)} %broadcast_in_dim.22), calls=%async_computation | async-start | bytes 65536 | tf_op jit(solution)/shard_map/all_to_all | solution.py:15
  13.6 8.4 %all-to-all-start.1 = ((bf16[4,4,128]{2,1,0:T(4,128)(2,1)}), bf16[4,4,128]{2,1,0:T(4,128)(2,1)S(1)}, u32[]{:S(2)}, u32[]{:S(2)}) async-start(bf16[4,4,128]{2,1,0:T(4,128)(2,1)} %convert_element_type.68), calls=%async_computation.1 | async-start | bytes 8192 | tf_op jit(solution)/shard_map/all_to_all | solution.py:124
  22.9 0.7 copy-start.7
  23.6 9.3 %copy-start.2 = (bf16[512,256]{1,0:T(8,128)(2,1)S(1)}, bf16[512,256]{1,0:T(8,128)(2,1)}, u32[]{:S(2)}) copy-start(bf16[512,256]{1,0:T(8,128)(2,1)} %param.26) | copy-start | bytes 786436
  24.0 0.7 copy-start.8
  25.3 3.4 %copy-start.5 = (s32[16,6]{0,1:T(8,128)S(1)}, s32[16,6]{0,1:T(8,128)}, u32[]{:S(2)}) copy-start(s32[16,6]{0,1:T(8,128)} %param.28) | copy-start | bytes 1156
  25.4 7.6 %all-to-all-start.2 = ((bf16[4,4,512]{2,1,0:T(4,128)(2,1)}), bf16[4,4,512]{2,1,0:T(4,128)(2,1)S(1)}, u32[]{:S(2)}, u32[]{:S(2)}) async-start(bf16[4,4,512]{2,1,0:T(4,128)(2,1)} %broadcast_in_dim.26), calls=%async_computation.2 | async-start | bytes 32768 | tf_op jit(solution)/shard_map/all_to_all | solution.py:15
  33.7 7.7 %all-to-all-start.3 = ((f32[4,16,256]{2,1,0:T(8,128)}), f32[4,16,256]{2,1,0:T(8,128)S(1)}, u32[]{:S(2)}, u32[]{:S(2)}) async-start(f32[4,16,256]{2,1,0:T(8,128)} %broadcast_in_dim.27), calls=%async_computation.3 | async-start | bytes 131072 | tf_op jit(solution)/shard_map/all_to_all | solution.py:15
  41.8 0.7 copy-start.6
  43.1 42.4 %copy-start.9 = (bf16[1,1024,256]{2,1,0:T(8,128)(2,1)S(1)}, bf16[1,1024,256]{2,1,0:T(8,128)(2,1)}, u32[]{:S(2)}) copy-start(bf16[1,1024,256]{2,1,0:T(8,128)(2,1)} %param.30) | copy-start | bytes 1572868
  85.5 1.0 copy-start.10
  85.5 1.2 copy-start.11
  88.2 3.6 %copy-start.4 = (f32[16,6]{0,1:T(8,128)S(1)}, f32[16,6]{0,1:T(8,128)}, u32[]{:S(2)}) copy-start(f32[16,6]{0,1:T(8,128)} %param.29) | copy-start | bytes 1156
  88.2 13.4 %all-to-all-start.5 = ((bf16[4,128,2,256]{3,1,2,0:T(8,128)(2,1)}), bf16[4,128,2,256]{3,1,2,0:T(8,128)(2,1)S(1)}, u32[]{:S(2)}, u32[]{:S(2)}) async-start(bf16[4,128,2,256]{3,1,2,0:T(8,128)(2,1)} %bitcast.101), calls=%async_computation.5 | async-start | bytes 1048576 | tf_op jit(solution)/shard_map/all_to_all | solution.py:37
  102.5 18.6 %all-to-all-start.6 = ((bf16[128,2,256]{2,1,0:T(2,128)(2,1)}), bf16[128,2,256]{2,1,0:T(2,128)(2,1)S(1)}, u32[]{:S(2)}, u32[]{:S(2)}) async-start(bf16[128,2,256]{2,1,0:T(2,128)(2,1)} %copy.115), calls=%async_computation.6 | async-start | bytes 262144 | tf_op jit(solution)/shard_map/all_to_all | solution.py:183
  122.2 7.3 %all-to-all-start.7 = ((f32[4,1,32]{2,1,0:T(1,128)}), f32[4,1,32]{2,1,0:T(1,128)S(1)}, u32[]{:S(2)}, u32[]{:S(2)}) async-start(f32[4,1,32]{2,1,0:T(1,128)} %broadcast_in_dim.28), calls=%async_computation.7 | async-start | bytes 4096 | tf_op jit(solution)/shard_map/all_to_all | solution.py:15
where the time goes:
time: 131 us; the launch traced here: 130 us
  blocking collectives  42.4 us (32%)
  waiting for transfers between devices  37.7 us (29%)
  starting transfers between devices  28.3 us (22%)
  local copies, waits for them, and re-layouts  12.4 us (9%)
  matrix products  4.71 us (4%)
  other arithmetic  4.47 us (3%)
    all_to_all x1, blocking collectives, body(): lax.all_to_all(outgoing, 'ep', split_axis=0, concat_axis=0, tiled=True)  42.4 us
    all_to_all x4, starting transfers between devices, copy_for_each(): lax.all_to_all(jnp.broadcast_to(x[None], (count, *x.shape)), axis, 0, 0,...  14.7 us
    all_to_all x1, waiting for transfers between devices, body(): lax.all_to_all(answers, 'ep', split_axis=0, concat_axis=0, tiled=True)  12.8 us
    all_to_all x4, waiting for transfers between devices, copy_for_each(): lax.all_to_all(jnp.broadcast_to(x[None], (count, *x.shape)), axis, 0, 0,...  11.7 us
    all_to_all x1, waiting for transfers between devices, sum_at_owner(): lax.all_to_all(pieces, axis, split_axis=0, concat_axis=0, tiled=True)  9.76 us
    all_to_all x1, starting transfers between devices, body(): lax.all_to_all(answers, 'ep', split_axis=0, concat_axis=0, tiled=True)  5.77 us
    unnamed x28, local copies, waits for them, and re-layouts  5.31 us
    all_to_all x1, starting transfers between devices, body(): lax.all_to_all(query, 'tp', split_axis=0, concat_axis=1, tiled=True)  4.23 us
  transfers between devices with their start and end apart: 7, of which 6 were waited for; matrix products, arithmetic and copies ran while one was open for 6% of the time, Pallas kernels for 0%

commit v1 on v0

--- a/solution.py
+++ b/solution.py
@@ -121,9 +121,9 @@
         group, -1, 2, head_dim
     )
     query = rotate(query, lengths).astype(bf16).reshape(group, -1)
-    query = lax.all_to_all(query, "tp", split_axis=0, concat_axis=1, tiled=True).reshape(
-        own, heads, 2, head_dim
-    )
+    query = jnp.concatenate(
+        lax.all_to_all(jnp.stack(jnp.split(query, lax.axis_size("tp"), axis=0)), "tp", 0, 0), axis=1
+    ).reshape(own, heads, 2, head_dim)
     own_lengths = lax.dynamic_slice_in_dim(lengths, tp_rank * own, own)
     new_key = jnp.dot(tokens, key_weight, preferred_element_type=f32).reshape(own, 2, head_dim)
     new_key = rotate(new_key, own_lengths).astype(bf16)

time: 131 us -> 131 us (level)
  no operation moved by 1% of the time
where the time goes in v1:
time: 131 us; the launch traced here: 130 us
  blocking collectives  42.4 us (32%)
  waiting for transfers between devices  37.7 us (29%)
  starting transfers between devices  28.3 us (22%)
  local copies, waits for them, and re-layouts  12 us (9%)
  other arithmetic  5.08 us (4%)
  matrix products  4.72 us (4%)
    all_to_all x1, blocking collectives, body(): lax.all_to_all(outgoing, 'ep', split_axis=0, concat_axis=0, tiled=True)  42.4 us
    all_to_all x4, starting transfers between devices, copy_for_each(): lax.all_to_all(jnp.broadcast_to(x[None], (count, *x.shape)), axis, 0, 0,...  14.7 us
    all_to_all x1, waiting for transfers between devices, body(): lax.all_to_all(answers, 'ep', split_axis=0, concat_axis=0, tiled=True)  12.8 us
    all_to_all x4, waiting for transfers between devices, copy_for_each(): lax.all_to_all(jnp.broadcast_to(x[None], (count, *x.shape)), axis, 0, 0,...  11.7 us
    all_to_all x1, waiting for transfers between devices, sum_at_owner(): lax.all_to_all(pieces, axis, split_axis=0, concat_axis=0, tiled=True)  9.76 us
    all_to_all x1, starting transfers between devices, body(): lax.all_to_all(answers, 'ep', split_axis=0, concat_axis=0, tiled=True)  5.77 us
    unnamed x28, local copies, waits for them, and re-layouts  5.31 us
    all_to_all x1, starting transfers between devices, body(): lax.all_to_all(jnp.stack(jnp.split(query, lax.axis_size('tp'), axis=0)),...  4.24 us
  transfers between devices with their start and end apart: 7, of which 6 were waited for; matrix products, arithmetic and copies ran while one was open for 6% of the time, Pallas kernels for 0%

profile of v1, /device:TPU:1, one launch (start us, length us, event | category | flops | bytes accessed | tf_op | source)
XLA Modules:
  0.0 130.5 jit_solution(17092558044857435666)
XLA Ops:
  0.0 1.5 %broadcast_in_dim.22 = bf16[4,4,1024]{2,1,0:T(4,128)(2,1)} broadcast(bf16[4,1024]{1,0:T(4,128)(2,1)} %param.17), dimensions={1,2} | broadcast | bytes 40960 | tf_op jit(solution)/shard_map/broadcast_in_dim | solution.py:15
  1.5 4.8 %all-to-all-start = ((bf16[4,4,1024]{2,1,0:T(4,128)(2,1)}), bf16[4,4,1024]{2,1,0:T(4,128)(2,1)S(1)}, u32[]{:S(2)}, u32[]{:S(2)}) async-start(bf16[4,4,1024]{2,1,0:T(4,128)(2,1)} %broadcast_in_dim.22), calls=%async_computation | async-start | bytes 65536 | tf_op jit(solution)/shard_map/all_to_all | solution.py:15
  6.3 0.7 convert_element_type.68
  7.0 0.7 fusion.57
  7.7 0.1 multiply_cosine_fusion
  7.8 0.1 multiply_cosine_fusion.1
  7.9 1.1 fusion.59
  9.1 0.1 reshape.291
  9.2 0.8 fusion.6
  10.1 0.8 copy.127
  10.8 0.1 eq.51
  10.9 0.1 fusion.34
  11.0 0.1 reduce_window_sum.11
  11.2 0.2 select_reduce_fusion
  11.4 1.1 copy.117
  12.5 0.2 convolution_bitcast_fusion
  12.8 0.1 fusion.47
  12.9 0.1 stack.15
  13.0 0.1 stack.16
  13.1 0.1 stack.17
  13.2 0.1 stack.18
  13.3 0.6 pad_maximum_fusion
  13.9 4.2 %all-to-all-start.1 = ((bf16[4,4,128]{2,1,0:T(4,128)(2,1)}), bf16[4,4,128]{2,1,0:T(4,128)(2,1)S(1)}, u32[]{:S(2)}, u32[]{:S(2)}) async-start(bf16[4,4,128]{2,1,0:T(4,128)(2,1)} %pad_maximum_fusion), calls=%async_computation.1 | async-start | bytes 8192 | tf_op jit(solution)/shard_map/all_to_all | solution.py:125
  18.2 0.5 copy.123
  18.8 0.1 copy.128
  18.9 3.4 %all-to-all-done.1 = bf16[4,4,128]{2,1,0:T(4,128)(2,1)S(1)} async-done(((bf16[4,4,128]{2,1,0:T(4,128)(2,1)}), bf16[4,4,128]{2,1,0:T(4,128)(2,1)S(1)}, u32[]{:S(2)}, u32[]{:S(2)}) %all-to-all-start.1) | async-done | bytes 4128 | tf_op jit(solution)/shard_map/all_to_all | solution.py:125
  22.3 0.1 reshape.306
  22.4 0.1 fusion.38
  22.5 0.3 fusion.58
  22.8 0.2 fusion.25
  23.1 0.1 fusion.24
  23.2 0.6 copy-done.7
  23.9 0.4 multiply_reduce_fusion.1
  24.3 0.7 copy-done.8
  25.0 0.6 broadcast_in_dim.26
  25.6 3.4 %all-to-all-start.2 = ((bf16[4,4,512]{2,1,0:T(4,128)(2,1)}), bf16[4,4,512]{2,1,0:T(4,128)(2,1)S(1)}, u32[]{:S(2)}, u32[]{:S(2)}) async-start(bf16[4,4,512]{2,1,0:T(4,128)(2,1)} %broadcast_in_dim.26), calls=%async_computation.2 | async-start | bytes 32768 | tf_op jit(solution)/shard_map/all_to_all | solution.py:15
  29.1 4.1 %all-to-all-done.2 = bf16[4,4,512]{2,1,0:T(4,128)(2,1)S(1)} async-done(((bf16[4,4,512]{2,1,0:T(4,128)(2,1)}), bf16[4,4,512]{2,1,0:T(4,128)(2,1)S(1)}, u32[]{:S(2)}, u32[]{:S(2)}) %all-to-all-start.2) | async-done | bytes 16416 | tf_op jit(solution)/shard_map/all_to_all | solution.py:15
  33.2 0.1 convolution_add_fusion
  33.4 0.6 broadcast_in_dim.27
  34.0 3.3 %all-to-all-start.3 = ((f32[4,16,256]{2,1,0:T(8,128)}), f32[4,16,256]{2,1,0:T(8,128)S(1)}, u32[]{:S(2)}, u32[]{:S(2)}) async-start(f32[4,16,256]{2,1,0:T(8,128)} %broadcast_in_dim.27), calls=%async_computation.3 | async-start | bytes 131072 | tf_op jit(solution)/shard_map/all_to_all | solution.py:15
  37.4 4.4 %all-to-all-done.3 = f32[4,16,256]{2,1,0:T(8,128)S(1)} async-done(((f32[4,16,256]{2,1,0:T(8,128)}), f32[4,16,256]{2,1,0:T(8,128)S(1)}, u32[]{:S(2)}, u32[]{:S(2)}) %all-to-all-start.3) | async-done | bytes 65568 | tf_op jit(solution)/shard_map/all_to_all | solution.py:15
  41.7 0.1 reduce_sum.115
  41.9 0.2 fusion.32
  42.1 0.7 copy-done.6
  42.8 0.3 convolution_convert_fusion.1
  43.2 0.2 reshape.294
  43.4 42.4 %all_to_all.41 = bf16[128,2,1024]{2,1,0:T(2,128)(2,1)S(1)} all-to-all(bf16[128,2,1024]{2,1,0:T(2,128)(2,1)S(1)} %reshape.294), channel_id=1, replica_groups=mesh['ep'=128,'tp'=4] {'ep'}, dimensions={0} | all-to-all | bytes 1048576 | tf_op jit(solution)/shard_map/all_to_all | solution.py:174
  85.8 0.3 convolution_minimum_fusion
  86.1 0.7 copy-done.10
  86.8 0.2 copy-done.11
  86.9 0.7 convolution_convert_fusion
  87.7 0.8 copy.159
  88.5 3.6 %all-to-all-start.5 = ((bf16[4,128,2,256]{3,1,2,0:T(8,128)(2,1)}), bf16[4,128,2,256]{3,1,2,0:T(8,128)(2,1)S(1)}, u32[]{:S(2)}, u32[]{:S(2)}) async-start(bf16[4,128,2,256]{3,1,2,0:T(8,128)(2,1)} %bitcast.107), calls=%async_computation.5 | async-start | bytes 1048576 | tf_op jit(solution)/shard_map/all_to_all | solution.py:37
  92.2 9.8 %all-to-all-done.5 = bf16[4,128,2,256]{3,1,2,0:T(8,128)(2,1)S(1)} async-done(((bf16[4,128,2,256]{3,1,2,0:T(8,128)(2,1)}), bf16[4,128,2,256]{3,1,2,0:T(8,128)(2,1)S(1)}, u32[]{:S(2)}, u32[]{:S(2)}) %all-to-all-start.5) | async-done | bytes 524320 | tf_op jit(solution)/shard_map/all_to_all | solution.py:37
  102.0 0.8 copy.133
  102.8 5.8 %all-to-all-start.6 = ((bf16[128,2,256]{2,1,0:T(2,128)(2,1)}), bf16[128,2,256]{2,1,0:T(2,128)(2,1)S(1)}, u32[]{:S(2)}, u32[]{:S(2)}) async-start(bf16[128,2,256]{2,1,0:T(2,128)(2,1)} %copy.133), calls=%async_computation.6 | async-start | bytes 262144 | tf_op jit(solution)/shard_map/all_to_all | solution.py:183
  108.6 12.8 %all-to-all-done.6 = bf16[128,2,256]{2,1,0:T(2,128)(2,1)S(1)} async-done(((bf16[128,2,256]{2,1,0:T(2,128)(2,1)}), bf16[128,2,256]{2,1,0:T(2,128)(2,1)S(1)}, u32[]{:S(2)}, u32[]{:S(2)}) %all-to-all-start.6) | async-done | bytes 131104 | tf_op jit(solution)/shard_map/all_to_all | solution.py:183
  121.4 0.2 fusion.5
  121.6 0.1 fusion.50
  121.9 0.6 broadcast_in_dim.28
  122.4 3.2 %all-to-all-start.7 = ((f32[4,1,32]{2,1,0:T(1,128)}), f32[4,1,32]{2,1,0:T(1,128)S(1)}, u32[]{:S(2)}, u32[]{:S(2)}) async-start(f32[4,1,32]{2,1,0:T(1,128)} %broadcast_in_dim.28), calls=%async_computation.7 | async-start | bytes 4096 | tf_op jit(solution)/shard_map/all_to_all | solution.py:15
  125.7 0.8 dynamic_slice.15
  126.4 3.3 %all-to-all-done.7 = f32[4,1,32]{2,1,0:T(1,128)S(1)} async-done(((f32[4,1,32]{2,1,0:T(1,128)}), f32[4,1,32]{2,1,0:T(1,128)S(1)}, u32[]{:S(2)}, u32[]{:S(2)}) %all-to-all-start.7) | async-done | bytes 544 | tf_op jit(solution)/shard_map/all_to_all | solution.py:15
  129.8 0.7 multiply_convert_fusion.1
  (53 shorter events, 1.2 us)
Async XLA Ops:
  0.0 23.9 %copy-start = (bf16[4,1024,128]{2,1,0:T(8,128)(2,1)S(1)}, bf16[4,1024,128]{2,1,0:T(8,128)(2,1)}, u32[]{:S(2)}) copy-start(bf16[4,1024,128]{2,1,0:T(8,128)(2,1)} %param.20) | copy-start | bytes 3145732
  0.0 9.2 %copy-start.3 = (bf16[1024,128]{1,0:T(8,128)(2,1)S(1)}, bf16[1024,128]{1,0:T(8,128)(2,1)}, u32[]{:S(2)}) copy-start(bf16[1024,128]{1,0:T(8,128)(2,1)} %param.23) | copy-start | bytes 786436
  0.0 18.2 %copy-start.1 = (bf16[4,1024,128]{2,1,0:T(8,128)(2,1)S(1)}, bf16[4,1024,128]{2,1,0:T(8,128)(2,1)}, u32[]{:S(2)}) copy-start(bf16[4,1024,128]{2,1,0:T(8,128)(2,1)} %param.19) | copy-start | bytes 3145732
  1.5 11.0 %all-to-all-start = ((bf16[4,4,1024]{2,1,0:T(4,128)(2,1)}), bf16[4,4,1024]{2,1,0:T(4,128)(2,1)S(1)}, u32[]{:S(2)}, u32[]{:S(2)}) async-start(bf16[4,4,1024]{2,1,0:T(4,128)(2,1)} %broadcast_in_dim.22), calls=%async_computation | async-start | bytes 65536 | tf_op jit(solution)/shard_map/all_to_all | solution.py:15
  13.9 8.4 %all-to-all-start.1 = ((bf16[4,4,128]{2,1,0:T(4,128)(2,1)}), bf16[4,4,128]{2,1,0:T(4,128)(2,1)S(1)}, u32[]{:S(2)}, u32[]{:S(2)}) async-start(bf16[4,4,128]{2,1,0:T(4,128)(2,1)} %pad_maximum_fusion), calls=%async_computation.1 | async-start | bytes 8192 | tf_op jit(solution)/shard_map/all_to_all | solution.py:125
  23.2 0.7 copy-start.7
  23.9 9.3 %copy-start.2 = (bf16[512,256]{1,0:T(8,128)(2,1)S(1)}, bf16[512,256]{1,0:T(8,128)(2,1)}, u32[]{:S(2)}) copy-start(bf16[512,256]{1,0:T(8,128)(2,1)} %param.26) | copy-start | bytes 786436
  24.3 0.7 copy-start.8
  25.6 3.4 %copy-start.5 = (s32[16,6]{0,1:T(8,128)S(1)}, s32[16,6]{0,1:T(8,128)}, u32[]{:S(2)}) copy-start(s32[16,6]{0,1:T(8,128)} %param.28) | copy-start | bytes 1156
  25.6 7.6 %all-to-all-start.2 = ((bf16[4,4,512]{2,1,0:T(4,128)(2,1)}), bf16[4,4,512]{2,1,0:T(4,128)(2,1)S(1)}, u32[]{:S(2)}, u32[]{:S(2)}) async-start(bf16[4,4,512]{2,1,0:T(4,128)(2,1)} %broadcast_in_dim.26), calls=%async_computation.2 | async-start | bytes 32768 | tf_op jit(solution)/shard_map/all_to_all | solution.py:15
  34.0 7.7 %all-to-all-start.3 = ((f32[4,16,256]{2,1,0:T(8,128)}), f32[4,16,256]{2,1,0:T(8,128)S(1)}, u32[]{:S(2)}, u32[]{:S(2)}) async-start(f32[4,16,256]{2,1,0:T(8,128)} %broadcast_in_dim.27), calls=%async_computation.3 | async-start | bytes 131072 | tf_op jit(solution)/shard_map/all_to_all | solution.py:15
  42.1 0.7 copy-start.6
  43.4 42.4 %copy-start.9 = (bf16[1,1024,256]{2,1,0:T(8,128)(2,1)S(1)}, bf16[1,1024,256]{2,1,0:T(8,128)(2,1)}, u32[]{:S(2)}) copy-start(bf16[1,1024,256]{2,1,0:T(8,128)(2,1)} %param.30) | copy-start | bytes 1572868
  85.7 1.0 copy-start.10
  85.8 1.2 copy-start.11
  88.5 3.6 %copy-start.4 = (f32[16,6]{0,1:T(8,128)S(1)}, f32[16,6]{0,1:T(8,128)}, u32[]{:S(2)}) copy-start(f32[16,6]{0,1:T(8,128)} %param.29) | copy-start | bytes 1156
  88.5 13.4 %all-to-all-start.5 = ((bf16[4,128,2,256]{3,1,2,0:T(8,128)(2,1)}), bf16[4,128,2,256]{3,1,2,0:T(8,128)(2,1)S(1)}, u32[]{:S(2)}, u32[]{:S(2)}) async-start(bf16[4,128,2,256]{3,1,2,0:T(8,128)(2,1)} %bitcast.107), calls=%async_computation.5 | async-start | bytes 1048576 | tf_op jit(solution)/shard_map/all_to_all | solution.py:37
  102.8 18.6 %all-to-all-start.6 = ((bf16[128,2,256]{2,1,0:T(2,128)(2,1)}), bf16[128,2,256]{2,1,0:T(2,128)(2,1)S(1)}, u32[]{:S(2)}, u32[]{:S(2)}) async-start(bf16[128,2,256]{2,1,0:T(2,128)(2,1)} %copy.133), calls=%async_computation.6 | async-start | bytes 262144 | tf_op jit(solution)/shard_map/all_to_all | solution.py:183
  122.4 7.3 %all-to-all-start.7 = ((f32[4,1,32]{2,1,0:T(1,128)}), f32[4,1,32]{2,1,0:T(1,128)S(1)}, u32[]{:S(2)}, u32[]{:S(2)}) async-start(f32[4,1,32]{2,1,0:T(1,128)} %broadcast_in_dim.28), calls=%async_computation.7 | async-start | bytes 4096 | tf_op jit(solution)/shard_map/all_to_all | solution.py:15
